TPU v7x, 32 devices: a whole 2x2x4 slice. The times are simulated.
32 devices in a mesh: sp: 8 (over z, y), dp: 4 (over x, core).
Axes of the slice: x: 2, y: 2, z: 4, core: 2. Of those that a mesh axis runs over, the one named last changes fastest.
Arguments:
- resid: bfloat16 [4, 2048, 2048], P('dp', 'sp'), may hold values from -6 to 6
- mixer_inputs: bfloat16 [4, 2048, 4096], P('dp', 'sp'), may hold values from -6 to 6
- output_gate: bfloat16 [4, 2048, 4096], P('dp', 'sp'), may hold values from -6 to 6
- write_rows_input: bfloat16 [4, 2048, 256], P('dp', 'sp'), may hold values from -6 to 6
- read_rows_input: bfloat16 [4, 2048, 256], P('dp', 'sp'), may hold values from -6 to 6
- step_size_logits: bfloat16 [4, 2048, 64, 2], P('dp', 'sp'), may hold values from -5 to 5
- extra_log_decay: bfloat16 [4, 2048, 64, 2], P('dp', 'sp'), may hold values from -0.7 to 0
- mixer_conv_taps: bfloat16 [5, 4096], P(None, 'sp'), may hold values from -2.5 to 2.5
- write_conv_taps: bfloat16 [5, 256], replicated, may hold values from -2.5 to 2.5
- read_conv_taps: bfloat16 [5, 256], replicated, may hold values from -2.5 to 2.5
- step_size_bias: float32 [64, 2], P('sp'), may hold values from -20 to -3
- decay_speed: float32 [64, 2], P('sp'), may hold values from 1 to 16
- grouped_norm_gain: float32 [4096], replicated, may hold values from 0.1 to 1.9
- output_matrix: bfloat16 [4096, 2048], P(None, 'dp'), may hold values from -0.09375 to 0.09375
- output_gain: float32 [2048], replicated, may hold values from 0.1 to 1.9
- feedforward_gain: float32 [2048], replicated, may hold values from 0.1 to 1.9
- routes: int32 [4, 2048, 2], P('dp', 'sp'), may hold values from 0 to 7, all different within a row; in each aligned block of 256 rows (0 to 255, 256 to 511, ..., all dimensions but the last counted through in order) at most 96 rows name the same one
- route_weights: float32 [4, 2048, 2], P('dp', 'sp'), may hold values from 0.1 to 1
- expert_gate_weight: bfloat16 [8, 2048, 1024], P('sp'), may hold values from -0.125 to 0.125
- expert_up_weight: bfloat16 [8, 2048, 1024], P('sp'), may hold values from -0.125 to 0.125
- expert_down_weight: bfloat16 [8, 1024, 2048], P('sp'), may hold values from -0.1875 to 0.1875
- expert_sum_gain: float32 [2048], replicated, may hold values from 0.1 to 1.9
Outputs:
- mixed_out: bfloat16 [4, 2048, 2048], P('dp', 'sp')
Inputs may be any that keep to these rules, and one draw needn't show every extreme that they name: `routes`: each token names 2 different experts; the 256 positions of one device name one expert at most 96 times, a bound that some block reaches.
All inputs are finite; a program needn't handle non-finite values.
Results may differ from a plain program's by a relative error of at most 0.012.
Values may be sent and summed in bfloat16 or wider, within the bound.
A program may use at most 128 MiB of HBM per device.

v0:
```python
import jax
import jax.numpy as jnp
from jax import lax
from jax.sharding import PartitionSpec as P

D = 2048
HEADS = 64
HEAD_DIM = 64
GROUPS = 2
STATE = 128
BLOCK = 128
TOPK = 2
INNER = 4096
EPS = 1e-06


def rms_scale(values, scale_gain):
    return values * lax.rsqrt(jnp.mean(values * values, axis=-1, keepdims=True) + EPS) * scale_gain


def centred_conv(values, kernel):
    span_len = kernel.shape[0]
    half_span = span_len // 2
    length = values.shape[0]
    padded = jnp.pad(values.astype(jnp.float32), ((half_span, half_span), (0, 0)))
    summed = jnp.zeros(values.shape, jnp.float32)
    for offset in range(span_len):
        summed = summed + padded[offset : offset + length] * kernel[offset].astype(jnp.float32)
    return jax.nn.silu(summed).astype(jnp.bfloat16)


def block_pass(inputs, writes, read_rows, head_step_sizes, logarithm_decay):
    length = inputs.shape[0]
    blocks = length // BLOCK
    inp_block = inputs.reshape(blocks, BLOCK, -1)
    wr_block = writes.reshape(blocks, BLOCK, -1)
    rd_block = read_rows.reshape(blocks, BLOCK, -1)
    step_blk = head_step_sizes.reshape(blocks, BLOCK)
    cumulative = jnp.cumsum(logarithm_decay.reshape(blocks, BLOCK), axis=1)
    lower_tri = jnp.tril(jnp.ones((BLOCK, BLOCK), dtype=bool))
    spread = cumulative[:, :, None] - cumulative[:, None, :]
    in_block = jnp.where(lower_tri, jnp.exp(jnp.where(lower_tri, spread, 0.0)), 0.0)
    scores = jnp.einsum("cln,csn->cls", rd_block, wr_block, preferred_element_type=jnp.float32)
    weights = (scores * in_block * step_blk[:, None, :]).astype(jnp.bfloat16)
    within = jnp.einsum("cls,csp->clp", weights, inp_block, preferred_element_type=jnp.float32)
    to_end = jnp.exp(cumulative[:, -1:] - cumulative) * step_blk
    scaled = (wr_block.astype(jnp.float32) * to_end[:, :, None]).astype(jnp.bfloat16)
    states = jnp.einsum("csn,csp->cnp", scaled, inp_block, preferred_element_type=jnp.float32)
    totals = cumulative[:, -1]
    through = jnp.cumsum(totals)
    preceding = through - totals
    strict = jnp.tril(jnp.ones((blocks, blocks), dtype=bool), -1)
    carry_mat = jnp.where(
        strict, jnp.exp(jnp.where(strict, preceding[:, None] - through[None, :], 0.0)), 0.0
    )
    entering = jnp.dot(carry_mat, states.reshape(blocks, -1), precision=lax.Precision.HIGHEST)
    entering = entering.reshape(states.shape).astype(jnp.bfloat16)
    carried = (
        jnp.einsum("cln,cnp->clp", rd_block, entering, preferred_element_type=jnp.float32)
        * jnp.exp(cumulative)[:, :, None]
    )
    return (within + carried).reshape(length, -1)


def both_ways(inputs, writes, read_rows, head_step_sizes, logarithm_decay):
    forward = block_pass(inputs, writes, read_rows, head_step_sizes[:, 0], logarithm_decay[:, 0])
    backward = block_pass(
        jnp.flip(inputs, 0),
        jnp.flip(writes, 0),
        jnp.flip(read_rows, 0),
        jnp.flip(head_step_sizes[:, 1], 0),
        jnp.flip(logarithm_decay[:, 1], 0),
    )
    return forward + jnp.flip(backward, 0)


def head_result(packed_head):
    return both_ways(*packed_head).astype(jnp.bfloat16)


def local(
    resid,
    mixer_inputs,
    output_gate,
    write_rows_input,
    read_rows_input,
    step_size_logits,
    extra_log_decay,
    mixer_conv_taps,
    write_conv_taps,
    read_conv_taps,
    step_size_bias,
    decay_speed,
    grouped_norm_gain,
    output_matrix,
    output_gain,
    feedforward_gain,
    routes,
    route_weights,
    expert_gate_weight,
    expert_up_weight,
    expert_down_weight,
    expert_sum_gain,
):
    tok_rows = mixer_inputs.shape[1]
    local_heads = step_size_bias.shape[0]
    per_group = HEADS // GROUPS
    first_head = lax.axis_index("sp") * local_heads
    group_id = first_head // per_group
    heads_x = mixer_inputs[0].reshape(tok_rows, HEADS, HEAD_DIM)
    shifted_inputs, shifted_step_pre, shifted_extra_decay = (
        lax.all_to_all(heads_x, "sp", split_axis=1, concat_axis=0, tiled=True),
        lax.all_to_all(step_size_logits[0], "sp", split_axis=1, concat_axis=0, tiled=True),
        lax.all_to_all(extra_log_decay[0], "sp", split_axis=1, concat_axis=0, tiled=True),
    )
    seq_len = shifted_inputs.shape[0]
    whole_write, whole_read = (
        lax.all_gather(write_rows_input[0], "sp", axis=0, tiled=True),
        lax.all_gather(read_rows_input[0], "sp", axis=0, tiled=True),
    )
    col_start = group_id * STATE
    write_act = centred_conv(
        lax.dynamic_slice_in_dim(whole_write, col_start, STATE, 1),
        lax.dynamic_slice_in_dim(write_conv_taps, col_start, STATE, 1),
    )
    read_act = centred_conv(
        lax.dynamic_slice_in_dim(whole_read, col_start, STATE, 1),
        lax.dynamic_slice_in_dim(read_conv_taps, col_start, STATE, 1),
    )
    write_heads = jnp.broadcast_to(write_act[:, None, :], (seq_len, local_heads, STATE))
    read_heads = jnp.broadcast_to(read_act[:, None, :], (seq_len, local_heads, STATE))
    x_act = centred_conv(shifted_inputs.reshape(seq_len, local_heads * HEAD_DIM), mixer_conv_taps)
    x_act = x_act.reshape(seq_len, local_heads, HEAD_DIM)
    head_step_sizes = jax.nn.softplus(shifted_step_pre.astype(jnp.float32) + step_size_bias)
    logarithm_decay = shifted_extra_decay.astype(jnp.float32) - decay_speed * head_step_sizes
    by_head = tuple(
        (
            jnp.moveaxis(item, 1, 0)
            for item in (x_act, write_heads, read_heads, head_step_sizes, logarithm_decay)
        )
    )
    head_outputs = jnp.moveaxis(lax.map(head_result, by_head), 0, 1)
    token_heads = lax.all_to_all(head_outputs, "sp", split_axis=0, concat_axis=1, tiled=True)
    gated_vals = token_heads.reshape(tok_rows, INNER).astype(jnp.float32) * jax.nn.silu(
        output_gate[0].astype(jnp.float32)
    )
    grouped = gated_vals.reshape(tok_rows, GROUPS, -1)
    grouped = grouped * lax.rsqrt(jnp.mean(grouped * grouped, axis=-1, keepdims=True) + EPS)
    normed = (grouped.reshape(tok_rows, -1) * grouped_norm_gain).astype(jnp.bfloat16)
    projected = jnp.dot(
        normed,
        lax.all_gather(output_matrix, "dp", axis=1, tiled=True),
        preferred_element_type=jnp.float32,
    )
    resid_one = (resid[0].astype(jnp.float32) + rms_scale(projected, output_gain)).astype(
        jnp.bfloat16
    )
    ffn_in = rms_scale(resid_one.astype(jnp.float32), feedforward_gain).astype(jnp.bfloat16)
    sp_size = lax.axis_size("sp")
    local_experts = expert_gate_weight.shape[0]
    experts = local_experts * sp_size
    capacity = 3 * tok_rows * TOPK // (2 * experts)
    flat_route = routes[0].reshape(-1)
    one_hot = (flat_route[:, None] == jnp.arange(experts, dtype=jnp.int32)[None, :]).astype(
        jnp.int32
    )
    earlier = jnp.cumsum(one_hot, axis=0) - one_hot
    slot_pos = jnp.sum(earlier * one_hot, axis=1)
    slot_dest = flat_route * capacity + slot_pos
    source_tok = jnp.arange(tok_rows * TOPK, dtype=jnp.int32) // TOPK
    slot_token = jnp.full((experts * capacity,), tok_rows, jnp.int32).at[slot_dest].set(source_tok)
    padded_in = jnp.concatenate([ffn_in, jnp.zeros((1, D), jnp.bfloat16)], axis=0)
    send_rows = padded_in[slot_token].reshape(sp_size, local_experts, capacity, D)
    arrived = lax.all_to_all(send_rows, "sp", split_axis=0, concat_axis=0, tiled=True)
    gate_part = jnp.einsum(
        "sekd,edh->sekh", arrived, expert_gate_weight, preferred_element_type=jnp.float32
    )
    up_part = jnp.einsum(
        "sekd,edh->sekh", arrived, expert_up_weight, preferred_element_type=jnp.float32
    )
    hidden = (jax.nn.silu(gate_part) * up_part).astype(jnp.bfloat16)
    expert_rows = jnp.einsum(
        "sekh,ehd->sekd", hidden, expert_down_weight, preferred_element_type=jnp.float32
    ).astype(jnp.bfloat16)
    returned = lax.all_to_all(expert_rows, "sp", split_axis=0, concat_axis=0, tiled=True)
    picked = returned.reshape(experts * capacity, D)[slot_dest]
    weighted = picked.astype(jnp.float32) * route_weights[0].reshape(-1)[:, None]
    combined = jnp.sum(weighted.reshape(tok_rows, TOPK, D), axis=1)
    mixed_out = resid_one.astype(jnp.float32) + rms_scale(combined, expert_sum_gain)
    return mixed_out.astype(jnp.bfloat16)[None]


def solution(mesh):
    in_specs = (
        P("dp", "sp", None),
        P("dp", "sp", None),
        P("dp", "sp", None),
        P("dp", "sp", None),
        P("dp", "sp", None),
        P("dp", "sp", None, None),
        P("dp", "sp", None, None),
        P(None, "sp"),
        P(),
        P(),
        P("sp", None),
        P("sp", None),
        P(),
        P(None, "dp"),
        P(),
        P(),
        P("dp", "sp", None),
        P("dp", "sp", None),
        P("sp", None, None),
        P("sp", None, None),
        P("sp", None, None),
        P(),
    )
    out_specs = P("dp", "sp", None)
    return jax.shard_map(local, mesh=mesh, in_specs=in_specs, out_specs=out_specs, check_vma=False)
```

profile of v0, /device:TPU:0, one launch (start us, length us, event | category | flops | bytes accessed | tf_op | source)
XLA Modules:
  0.0 578.3 jit_solution(10283695238567507477)
XLA Ops:
  8.0 14.2 %all_to_all.46 = bf16[256,64,2]{0,2,1:T(2,128)(2,1)S(1)} all-to-all(bf16[256,64,2]{0,2,1:T(2,128)(2,1)} %bitcast.401), channel_id=1, replica_groups=mesh['sp'=8,'dp'=4] {'sp'}, dimensions={1} | all-to-all | bytes 131072 | tf_op jit(solution)/shard_map/all_to_all | solution.py:114
  22.2 3.4 all-to-all-start.1
  25.6 4.1 copy.122
  29.7 2.8 all-to-all-done.1
  32.5 3.6 all-to-all-start.2
  38.6 24.9 %all-gather.10.cloned.1.call-done = bf16[1,2048,256]{2,1,0:T(8,128)(2,1)} async-done(((bf16[1,256,256]{2,1,0:T(8,128)(2,1)}), bf16[1,2048,256]{2,1,0:T(8,128)(2,1)}) %all-gather.10.cloned.1.call-update) | async-done | bytes 1048592 | tf_op jit(solution)/shard_map/all_gather | solution.py:118
  63.5 50.5 %all-gather.8.cloned.1.call-done = bf16[1,2048,256]{2,1,0:T(8,128)(2,1)} async-done(((bf16[1,256,256]{2,1,0:T(8,128)(2,1)}), bf16[1,2048,256]{2,1,0:T(8,128)(2,1)}) %all-gather.8.cloned.1.call-update) | async-done | bytes 1048592 | tf_op jit(solution)/shard_map/all_gather | solution.py:119
  118.1 2.0 copy.142
  120.1 6.8 %multiply_convert_fusion.4 = bf16[2048,512]{0,1:T(8,128)(2,1)} fusion(f32[2048,512]{0,1:T(8,128)S(1)} %bitcast.384, f32[512]{0:T(512)S(1)} %bitcast.406, f32[512]{0:T(512)S(1)} %bitcast.407, f32[512]{0:T(512)S(1)} %bitcast.404, f32[512]{0:T(512)S(1)} %bitcast.405, f32[512]{0:T(512)S(1)} %bitcast.403), kind=kLoop, calls=%fused_computation.110 | loop fusion | flops 14680064 | bytes 6301696 | tf_op jit(solution)/shard_map/convert_element_type | solution.py:29
  126.9 3.0 transpose.107
  129.9 2.6 transpose.108
  132.5 142.8 %while.10 = (s32[]{:T(128)}, bf16[8,2048,64]{1,2,0:T(8,128)(2,1)}, bf16[8,2048,128]{2,1,0:T(8,128)(2,1)}, bf16[8,2048,128]{2,1,0:T(8,128)(2,1)}, f32[8,2048,2]{1...) while((s32[]{:T(128)}, bf16[8,2048,64]{1,2,0:T(8,128)(2,1)}, ...), condition=%wide.region_5.6_spmd, body=%wide.region_0.5_spmd.sunk | while | flops 392190464 | bytes 29739348 | solution.py:142
  139.4 1.6 fusion.190
  142.5 1.4 rev.32
  157.3 1.6 fusion.190
  160.4 1.4 rev.32
  175.2 1.6 fusion.190
  178.2 1.4 rev.32
  193.0 1.6 fusion.190
  210.9 1.6 fusion.190
  228.7 1.6 fusion.190
  246.5 1.6 fusion.190
  264.4 1.6 fusion.190
  275.4 5.6 copy.124
  281.0 7.6 %reshape.357 = bf16[8,2,65536]{2,1,0:T(2,128)(2,1)} reshape(bf16[2048,8,64]{2,1,0:T(8,128)(2,1)} %bitcast.383) | data formatting | bytes 4194304
  288.5 4.7 all-to-all-start.3
  293.7 3.3 copy.127
  297.0 2.5 convert.66
  301.3 2.4 scatter_custom_fusion
  303.7 36.9 %all-to-all-done.3 = bf16[8,2,65536]{2,1,0:T(2,128)(2,1)} async-done(((bf16[8,2,65536]{2,1,0:T(2,128)(2,1)}), bf16[8,2,65536]{2,1,0:T(2,128)(2,1)}, u32[]{:S(2)}, u32[]{:S(2)}) %all-to-all-start.3) | async-done | bytes 2097184 | tf_op jit(solution)/shard_map/all_to_all | solution.py:143
  340.6 7.4 %reshape.358 = bf16[2048,8,64]{2,1,0:T(8,128)(2,1)} reshape(bf16[8,2,65536]{2,1,0:T(2,128)(2,1)} %all-to-all-done.3) | data formatting | bytes 4194304
  348.0 5.5 copy.125
  353.5 2.1 convert_element_type.256
  355.6 2.0 copy.143
  357.6 2.0 copy-done
  359.6 3.4 multiply_reduce_fusion.1
  363.0 3.5 copy.126
  366.6 2.8 fusion.72
  369.4 9.4 %multiply_reduce_fusion.3 = (f32[256]{0:T(256)S(1)}, f32[256,2048]{1,0:T(8,128)S(1)}) fusion(bf16[256,4096]{0,1:T(8,128)(2,1)} %fusion.72, bf16[4096,2048]{1,0:T(8,128)(2,1)} %all-gather.6.cloned.1.call-done), kind=kOutput, calls=%fused_computation.134 | convolution fusion | flops 4296015872 | bytes 20972544 | tf_op jit(solution)/shard_map/dot_general | solution.py:150
  380.8 4.3 gather_fusion
  385.1 74.7 %all_to_all.47 = bf16[8,1,96,2048]{3,2,1,0:T(8,128)(2,1)S(1)} all-to-all(bf16[8,1,96,2048]{3,2,1,0:T(8,128)(2,1)} %bitcast.387), channel_id=1, replica_groups=mesh['sp'=8,'dp'=4] {'sp'}, dimensions={0} | all-to-all | bytes 6291456 | tf_op jit(solution)/shard_map/all_to_all | solution.py:174
  459.8 5.1 fusion.67
  465.0 13.0 %fusion.87 = bf16[8,1,96,2048]{3,2,1,0:T(8,128)(2,1)} fusion(bf16[1,1024,2048]{2,1,0:T(8,128)(2,1)} %param.44, f32[8,96,1024]{2,1,0:T(8,128)} %fusion.67, bf16[1,2048,1024]{2,1,0:T(8,128)(2,1)} %param.42, bf16[8,1,96,2048]{3,2,1,0:T(8,128)(2,1)S(1)} %all_to_all.47), kind=kOutput, calls=%fused_computation.126 | convolution fusion | flops 6448742400 | bytes 17825792 | tf_op jit(solution)/shard_map/sekh,ehd->sekd/dot_general | solution.py:182
  478.0 4.0 all-to-all-start.5
  482.1 70.1 %all-to-all-done.5 = bf16[8,1,96,2048]{3,2,1,0:T(8,128)(2,1)S(1)} async-done(((bf16[8,1,96,2048]{3,2,1,0:T(8,128)(2,1)}), bf16[8,1,96,2048]{3,2,1,0:T(8,128)(2,1)S(1)}, u32[]{:S(2)}, u32[]{:S(2)}) %all-to-all-start.5) | async-done | bytes 3145760 | tf_op jit(solution)/shard_map/all_to_all | solution.py:185
  552.3 3.3 gather_fusion.1
  555.6 5.4 reshape.306
  561.0 9.0 %multiply_reduce_fusion = f32[256,2048]{1,0:T(8,128)S(1)} fusion(f32[256,2,2048]{2,1,0:T(2,128)} %reshape.306, f32[256,2]{1,0:T(8,128)S(1)} %copy.135), kind=kLoop, calls=%fused_computation.108 | loop fusion | flops 1572864 | bytes 6293504 | tf_op jit(solution)/shard_map/reduce_sum | solution.py:188
  (411 shorter events, 138.2 us)
Async XLA Ops:
  6.5 56.9 %all-gather.10.cloned.1.call-start = ((), (), s32[]{:S(2)}) async-start(), calls=%async_computation.8 | async-start | bytes 1179648 | tf_op jit(solution)/shard_map/all_gather | solution.py:118
  7.3 106.7 %all-gather.8.cloned.1.call-start = ((), (), s32[]{:S(2)}) async-start(), calls=%async_computation.7 | async-start | bytes 1179648 | tf_op jit(solution)/shard_map/all_gather | solution.py:119
  22.2 10.3 %all-to-all-start.1 = ((bf16[256,64,2]{0,2,1:T(2,128)(2,1)}), bf16[256,64,2]{0,2,1:T(2,128)(2,1)S(1)}, u32[]{:S(2)}, u32[]{:S(2)}) async-start(bf16[256,64,2]{0,2,1:T(2,128)(2,1)} %bitcast.402), calls=%async_computation.1 | async-start | bytes 131072 | tf_op jit(solution)/shard_map/all_to_all | solution.py:113
  32.5 84.4 %all-to-all-start.2 = ((bf16[256,64,64]{0,2,1:T(8,128)(2,1)}), bf16[256,64,64]{0,2,1:T(8,128)(2,1)S(1)}, u32[]{:S(2)}, u32[]{:S(2)}) async-start(bf16[256,64,64]{0,2,1:T(8,128)(2,1)} %bitcast.389), calls=%async_computation.2 | async-start | bytes 4194304 | tf_op jit(solution)/shard_map/all_to_all | solution.py:112
  36.1 0.8 copy-start.15
  36.1 0.9 copy-start.16
  36.1 1.0 copy-start.13
  36.2 1.0 copy-start.14
  36.2 1.0 copy-start.7
  36.2 333.2 %all-gather.6.cloned.1.call-start = ((), (), s32[]{:S(2)}) async-start(), calls=%async_computation.6 | async-start | bytes 20971520 | tf_op jit(solution)/shard_map/all_gather | solution.py:152
  147.4 2.2 copy-start.2
  165.3 2.2 copy-start.2
  183.2 2.2 copy-start.2
  201.0 2.2 copy-start.2
  218.9 2.2 copy-start.2
  236.7 2.2 copy-start.2
  254.5 2.2 copy-start.2
  272.4 2.2 copy-start.2
  288.5 4.7 copy-start.11
  288.5 52.0 %all-to-all-start.3 = ((bf16[8,2,65536]{2,1,0:T(2,128)(2,1)}), bf16[8,2,65536]{2,1,0:T(2,128)(2,1)}, u32[]{:S(2)}, u32[]{:S(2)}) async-start(bf16[8,2,65536]{2,1,0:T(2,128)(2,1)} %reshape.357), calls=%async_computation.3 | async-start | bytes 4194304 | tf_op jit(solution)/shard_map/all_to_all | solution.py:143
  355.6 4.0 copy-start.1
  357.6 2.0 copy-start
  363.0 3.6 copy-start.6
  369.4 9.4 %copy-start.5 = (bf16[1,256,2048]{2,1,0:T(8,128)(2,1)S(1)}, bf16[1,256,2048]{2,1,0:T(8,128)(2,1)}, u32[]{:S(2)}) copy-start(bf16[1,256,2048]{2,1,0:T(8,128)(2,1)} %param.24) | copy-start | bytes 3145732
  369.4 9.4 %copy-start.8 = (f32[2048]{0:T(1024)S(1)}, f32[2048]{0:T(1024)}, u32[]{:S(2)}) copy-start(f32[2048]{0:T(1024)} %param.38) | copy-start | bytes 24580
  378.8 1.6 copy-start.9
  379.5 1.0 copy-start.3
  385.1 74.7 %copy-start.17 = (bf16[1,2048,1024]{2,1,0:T(8,128)(2,1)S(1)}, bf16[1,2048,1024]{2,1,0:T(8,128)(2,1)}, u32[]{:S(2)}) copy-start(bf16[1,2048,1024]{2,1,0:T(8,128)(2,1)} %param.43) | copy-start | bytes 12582916
  478.0 4.0 copy-start.12
  478.0 74.3 %all-to-all-start.5 = ((bf16[8,1,96,2048]{3,2,1,0:T(8,128)(2,1)}), bf16[8,1,96,2048]{3,2,1,0:T(8,128)(2,1)S(1)}, u32[]{:S(2)}, u32[]{:S(2)}) async-start(bf16[8,1,96,2048]{3,2,1,0:T(8,128)(2,1)} %fusion.87), calls=%async_computation.5 | async-start | bytes 6291456 | tf_op jit(solution)/shard_map/all_to_all | solution.py:185
  561.0 9.2 %copy-start.4 = (bf16[256,2048]{1,0:T(8,128)(2,1)S(1)}, bf16[256,2048]{1,0:T(8,128)(2,1)}, u32[]{:S(2)}) copy-start(bf16[256,2048]{1,0:T(8,128)(2,1)} %copy-done.3) | copy-start | bytes 3145732
  561.0 9.2 %copy-start.10 = (f32[2048]{0:T(1024)S(1)}, f32[2048]{0:T(1024)}, u32[]{:S(2)}) copy-start(f32[2048]{0:T(1024)} %param.45) | copy-start | bytes 24580
Sparse Core Ops, SparseCore 0:
  9.5 53.9 all-gather.9
  65.6 48.3 all-gather.7
  115.5 104.5 all-gather.5
where the time goes:
time: 586 us; the launch traced here: 578 us
  waiting for transfers between devices  187 us (32%)
  local copies, waits for them, and re-layouts  144 us (25%)
  blocking collectives  89 us (15%)
  matrix products  77.1 us (13%)
  other arithmetic  50.6 us (9%)
  starting transfers between devices  15.7 us (3%)
  between operations  13.8 us (2%)
    all_to_all x1, blocking collectives, local(): lax.all_to_all(send_rows, 'sp', split_axis=0, concat_axis=0, tiled=True)  74.7 us
    all_to_all x1, waiting for transfers between devices, local(): lax.all_to_all(expert_rows, 'sp', split_axis=0, concat_axis=0, tiled=True)  70.1 us
    all_gather x1, waiting for transfers between devices, local(): lax.all_gather(read_rows_input[0], 'sp', axis=0, tiled=True)  50.5 us
    all_to_all x1, waiting for transfers between devices, local(): lax.all_to_all(head_outputs, 'sp', split_axis=0, concat_axis=1, tiled=True)  36.9 us
    unnamed x43, local copies, waits for them, and re-layouts  29.6 us
    all_gather x1, waiting for transfers between devices, local(): lax.all_gather(write_rows_input[0], 'sp', axis=0, tiled=True)  24.9 us
    dot_general x16, matrix products, block_pass(): jnp.einsum('cls,csp->clp', weights, inp_block, preferred_element_type=jnp...  19.8 us
    all_to_all x1, blocking collectives, local(): lax.all_to_all(extra_log_decay[0], 'sp', split_axis=1, concat_axis=0, til...  14.2 us
  transfers between devices with their start and end apart: 7, of which 5 were waited for; matrix products, arithmetic and copies ran while one was open for 37% of the time, Pallas kernels for 0%

commit v1 on v0

--- a/solution.py
+++ b/solution.py
@@ -140,7 +140,10 @@
         )
     )
     head_outputs = jnp.moveaxis(lax.map(head_result, by_head), 0, 1)
-    token_heads = lax.all_to_all(head_outputs, "sp", split_axis=0, concat_axis=1, tiled=True)
+    token_heads = jnp.concatenate(
+        lax.all_to_all(jnp.stack(jnp.split(head_outputs, lax.axis_size("sp"), axis=0)), "sp", 0, 0),
+        axis=1,
+    )
     gated_vals = token_heads.reshape(tok_rows, INNER).astype(jnp.float32) * jax.nn.silu(
         output_gate[0].astype(jnp.float32)
     )

time: 586 us -> 563 us (0.961)
  local copies, waits for them, and re-layouts: 144 us -> 125 us
    unnamed x43, local copies, waits for them, and re-layouts: 29.6 us -> 23.2 us
    while x33 -> x32, local copies, waits for them, and re-layouts: 14.1 us -> 8.43 us
  transfers between devices with their start and end apart: 7 -> 7, of which waited for: 5 -> 5; matrix products, arithmetic and copies ran while one was open for 37% -> 35% of each run, Pallas kernels for 0% -> 0%
where the time goes in v1:
time: 563 us; the launch traced here: 556 us
  waiting for transfers between devices  189 us (34%)
  local copies, waits for them, and re-layouts  125 us (22%)
  blocking collectives  89.2 us (16%)
  matrix products  76.6 us (14%)
  other arithmetic  47 us (8%)
  starting transfers between devices  15 us (3%)
  between operations  13.8 us (2%)
    all_to_all x1, blocking collectives, local(): lax.all_to_all(send_rows, 'sp', split_axis=0, concat_axis=0, tiled=True)  74.9 us
    all_to_all x1, waiting for transfers between devices, local(): lax.all_to_all(expert_rows, 'sp', split_axis=0, concat_axis=0, tiled=True)  70.1 us
    all_gather x1, waiting for transfers between devices, local(): lax.all_gather(read_rows_input[0], 'sp', axis=0, tiled=True)  50.5 us
    all_to_all x1, waiting for transfers between devices, local(): lax.all_to_all(jnp.stack(jnp.split(head_outputs, lax.axis_size('sp'), axi...  38.1 us
    all_gather x1, waiting for transfers between devices, local(): lax.all_gather(write_rows_input[0], 'sp', axis=0, tiled=True)  24.9 us
    unnamed x43, local copies, waits for them, and re-layouts  23.2 us
    dot_general x16, matrix products, block_pass(): jnp.einsum('cls,csp->clp', weights, inp_block, preferred_element_type=jnp...  19.8 us
    all_to_all x1, blocking collectives, local(): lax.all_to_all(extra_log_decay[0], 'sp', split_axis=1, concat_axis=0, til...  14.2 us
  transfers between devices with their start and end apart: 7, of which 5 were waited for; matrix products, arithmetic and copies ran while one was open for 35% of the time, Pallas kernels for 0%

profile of v1, /device:TPU:0, one launch (start us, length us, event | category | flops | bytes accessed | tf_op | source)
XLA Modules:
  0.0 555.8 jit_solution(7177205188583301503)
XLA Ops:
  8.0 14.2 %all_to_all.42 = bf16[256,64,2]{0,2,1:T(2,128)(2,1)S(1)} all-to-all(bf16[256,64,2]{0,2,1:T(2,128)(2,1)} %bitcast.433), channel_id=1, replica_groups=mesh['sp'=8,'dp'=4] {'sp'}, dimensions={1} | all-to-all | bytes 131072 | tf_op jit(solution)/shard_map/all_to_all | solution.py:114
  22.2 3.4 all-to-all-start.1
  25.6 4.1 copy.63
  29.7 2.8 all-to-all-done.1
  32.5 3.6 all-to-all-start.2
  38.6 24.9 %all-gather.10.cloned.1.call-done = bf16[1,2048,256]{2,1,0:T(8,128)(2,1)} async-done(((bf16[1,256,256]{2,1,0:T(8,128)(2,1)}), bf16[1,2048,256]{2,1,0:T(8,128)(2,1)}) %all-gather.10.cloned.1.call-update) | async-done | bytes 1048592 | tf_op jit(solution)/shard_map/all_gather | solution.py:118
  63.5 50.5 %all-gather.8.cloned.1.call-done = bf16[1,2048,256]{2,1,0:T(8,128)(2,1)} async-done(((bf16[1,256,256]{2,1,0:T(8,128)(2,1)}), bf16[1,2048,256]{2,1,0:T(8,128)(2,1)}) %all-gather.8.cloned.1.call-update) | async-done | bytes 1048592 | tf_op jit(solution)/shard_map/all_gather | solution.py:119
  118.1 2.0 copy.78
  120.1 7.1 %multiply_convert_fusion.4 = bf16[2048,512]{0,1:T(8,128)(2,1)} fusion(f32[2048,512]{0,1:T(8,128)S(1)} %bitcast.409, f32[512]{0:T(512)S(1)} %bitcast.438, f32[512]{0:T(512)S(1)} %bitcast.439, f32[512]{0:T(512)S(1)} %bitcast.436, f32[512]{0:T(512)S(1)} %bitcast.437, f32[512]{0:T(512)S(1)} %bitcast.435), kind=kLoop, calls=%fused_computation.112 | loop fusion | flops 14680064 | bytes 6301696 | tf_op jit(solution)/shard_map/convert_element_type | solution.py:29
  127.2 3.3 transpose.107
  130.5 2.5 transpose.108
  133.0 142.8 %while.10 = (s32[]{:T(128)}, bf16[8,2048,64]{1,2,0:T(8,128)(2,1)}, bf16[8,2048,128]{2,1,0:T(8,128)(2,1)}, bf16[8,2048,128]{2,1,0:T(8,128)(2,1)}, f32[8,2048,2]{1...) while((s32[]{:T(128)}, bf16[8,2048,64]{1,2,0:T(8,128)(2,1)}, ...), condition=%wide.region_5.6_spmd, body=%wide.region_0.5_spmd.sunk | while | flops 392190464 | bytes 29739348 | solution.py:142
  139.9 1.6 fusion.200
  142.9 1.4 rev.32
  157.8 1.6 fusion.200
  160.8 1.4 rev.32
  175.6 1.6 fusion.200
  178.6 1.4 rev.32
  193.5 1.6 fusion.200
  196.5 1.4 rev.32
  211.3 1.6 fusion.200
  229.1 1.6 fusion.200
  247.0 1.6 fusion.200
  264.8 1.6 fusion.200
  275.8 1.7 fusion.120
  277.4 1.7 fusion.119
  279.1 1.7 fusion.118
  280.8 1.7 fusion.117
  282.4 1.7 fusion.116
  284.1 1.7 fusion.115
  285.8 1.7 fusion.114
  287.5 1.7 fusion.113
  289.2 3.9 all-to-all-start.3
  293.5 4.1 copy.65
  299.4 2.4 scatter_custom_fusion
  301.9 38.1 %all-to-all-done.3 = bf16[8,256,8,64]{1,3,2,0:T(8,128)(2,1)S(1)} async-done(((bf16[8,256,8,64]{1,3,2,0:T(8,128)(2,1)}), bf16[8,256,8,64]{1,3,2,0:T(8,128)(2,1)S(1)}, u32[]{:S(2)}, u32[]{:S(2)}) %all-to-all-start.3) | async-done | bytes 2097184 | tf_op jit(solution)/shard_map/all_to_all | solution.py:144
  340.0 3.2 fusion.78
  343.2 3.7 fusion.67
  347.0 9.0 %multiply_reduce_fusion.2 = (f32[256]{0:T(256)S(1)}, f32[256,2048]{1,0:T(8,128)S(1)}) fusion(bf16[256,4096]{0,1:T(8,128)(2,1)} %fusion.67, bf16[4096,2048]{1,0:T(8,128)(2,1)} %all-gather.6.cloned.1.call-done), kind=kOutput, calls=%fused_computation.136 | convolution fusion | flops 4296015872 | bytes 20972544 | tf_op jit(solution)/shard_map/dot_general | solution.py:153
  358.0 4.3 gather_fusion
  362.3 74.9 %all_to_all.43 = bf16[8,1,96,2048]{3,2,1,0:T(8,128)(2,1)S(1)} all-to-all(bf16[8,1,96,2048]{3,2,1,0:T(8,128)(2,1)} %bitcast.411), channel_id=1, replica_groups=mesh['sp'=8,'dp'=4] {'sp'}, dimensions={0} | all-to-all | bytes 6291456 | tf_op jit(solution)/shard_map/all_to_all | solution.py:177
  437.2 5.1 fusion.70
  442.3 13.0 %fusion.89 = bf16[8,1,96,2048]{3,2,1,0:T(8,128)(2,1)} fusion(bf16[1,1024,2048]{2,1,0:T(8,128)(2,1)} %param.44, f32[8,96,1024]{2,1,0:T(8,128)} %fusion.70, bf16[1,2048,1024]{2,1,0:T(8,128)(2,1)} %param.42, bf16[8,1,96,2048]{3,2,1,0:T(8,128)(2,1)S(1)} %all_to_all.43), kind=kOutput, calls=%fused_computation.128 | convolution fusion | flops 6448742400 | bytes 17825792 | tf_op jit(solution)/shard_map/sekh,ehd->sekd/dot_general | solution.py:185
  455.3 4.1 all-to-all-start.5
  459.5 70.1 %all-to-all-done.5 = bf16[8,1,96,2048]{3,2,1,0:T(8,128)(2,1)S(1)} async-done(((bf16[8,1,96,2048]{3,2,1,0:T(8,128)(2,1)}), bf16[8,1,96,2048]{3,2,1,0:T(8,128)(2,1)S(1)}, u32[]{:S(2)}, u32[]{:S(2)}) %all-to-all-start.5) | async-done | bytes 3145760 | tf_op jit(solution)/shard_map/all_to_all | solution.py:188
  529.7 3.3 gather_fusion.1
  533.0 5.4 reshape.301
  538.4 9.0 %multiply_reduce_fusion = f32[256,2048]{1,0:T(8,128)S(1)} fusion(f32[256,2,2048]{2,1,0:T(2,128)} %reshape.301, f32[256,2]{1,0:T(8,128)S(1)} %copy.71), kind=kLoop, calls=%fused_computation.111 | loop fusion | flops 1572864 | bytes 6293504 | tf_op jit(solution)/shard_map/reduce_sum | solution.py:191
  (407 shorter events, 136.8 us)
Async XLA Ops:
  6.5 56.9 %all-gather.10.cloned.1.call-start = ((), (), s32[]{:S(2)}) async-start(), calls=%async_computation.8 | async-start | bytes 1179648 | tf_op jit(solution)/shard_map/all_gather | solution.py:118
  7.3 106.7 %all-gather.8.cloned.1.call-start = ((), (), s32[]{:S(2)}) async-start(), calls=%async_computation.7 | async-start | bytes 1179648 | tf_op jit(solution)/shard_map/all_gather | solution.py:119
  22.2 10.3 %all-to-all-start.1 = ((bf16[256,64,2]{0,2,1:T(2,128)(2,1)}), bf16[256,64,2]{0,2,1:T(2,128)(2,1)S(1)}, u32[]{:S(2)}, u32[]{:S(2)}) async-start(bf16[256,64,2]{0,2,1:T(2,128)(2,1)} %bitcast.434), calls=%async_computation.1 | async-start | bytes 131072 | tf_op jit(solution)/shard_map/all_to_all | solution.py:113
  32.5 84.4 %all-to-all-start.2 = ((bf16[256,64,64]{0,2,1:T(8,128)(2,1)}), bf16[256,64,64]{0,2,1:T(8,128)(2,1)S(1)}, u32[]{:S(2)}, u32[]{:S(2)}) async-start(bf16[256,64,64]{0,2,1:T(8,128)(2,1)} %bitcast.413), calls=%async_computation.2 | async-start | bytes 4194304 | tf_op jit(solution)/shard_map/all_to_all | solution.py:112
  36.1 0.8 copy-start.13
  36.1 0.9 copy-start.14
  36.1 1.0 copy-start.11
  36.2 1.0 copy-start.12
  36.2 1.0 copy-start.5
  36.2 310.8 %all-gather.6.cloned.1.call-start = ((), (), s32[]{:S(2)}) async-start(), calls=%async_computation.6 | async-start | bytes 20971520 | tf_op jit(solution)/shard_map/all_gather | solution.py:155
  147.9 2.2 copy-start
  165.8 2.2 copy-start
  183.6 2.2 copy-start
  201.5 2.2 copy-start
  219.3 2.2 copy-start
  237.1 2.2 copy-start
  255.0 2.2 copy-start
  272.8 2.2 copy-start
  282.4 10.6 %copy-start.9 = (s32[1,256,2]{1,2,0:T(2,128)S(1)}, s32[1,256,2]{1,2,0:T(2,128)}, u32[]{:S(2)}) copy-start(s32[1,256,2]{1,2,0:T(2,128)} %param.40) | copy-start | bytes 6148
  289.2 50.8 %all-to-all-start.3 = ((bf16[8,256,8,64]{1,3,2,0:T(8,128)(2,1)}), bf16[8,256,8,64]{1,3,2,0:T(8,128)(2,1)S(1)}, u32[]{:S(2)}, u32[]{:S(2)}) async-start(bf16[8,256,8,64]{1,3,2,0:T(8,128)(2,1)} %fusion.113), calls=%async_computation.3 | async-start | bytes 4194304 | tf_op jit(solution)/shard_map/all_to_all | solution.py:144
  297.6 45.6 %copy-start.4 = (f32[4096]{0:T(1024)S(1)}, f32[4096]{0:T(1024)}, u32[]{:S(2)}) copy-start(f32[4096]{0:T(1024)} %param.36) | copy-start | bytes 49156
  347.0 9.0 %copy-start.3 = (bf16[1,256,2048]{2,1,0:T(8,128)(2,1)S(1)}, bf16[1,256,2048]{2,1,0:T(8,128)(2,1)}, u32[]{:S(2)}) copy-start(bf16[1,256,2048]{2,1,0:T(8,128)(2,1)} %param.24) | copy-start | bytes 3145732
  347.0 9.0 %copy-start.6 = (f32[2048]{0:T(1024)S(1)}, f32[2048]{0:T(1024)}, u32[]{:S(2)}) copy-start(f32[2048]{0:T(1024)} %param.38) | copy-start | bytes 24580
  356.0 1.6 copy-start.7
  356.6 1.0 copy-start.1
  362.2 74.9 %copy-start.15 = (bf16[1,2048,1024]{2,1,0:T(8,128)(2,1)S(1)}, bf16[1,2048,1024]{2,1,0:T(8,128)(2,1)}, u32[]{:S(2)}) copy-start(bf16[1,2048,1024]{2,1,0:T(8,128)(2,1)} %param.43) | copy-start | bytes 12582916
  455.3 4.1 copy-start.10
  455.3 74.4 %all-to-all-start.5 = ((bf16[8,1,96,2048]{3,2,1,0:T(8,128)(2,1)}), bf16[8,1,96,2048]{3,2,1,0:T(8,128)(2,1)S(1)}, u32[]{:S(2)}, u32[]{:S(2)}) async-start(bf16[8,1,96,2048]{3,2,1,0:T(8,128)(2,1)} %fusion.89), calls=%async_computation.5 | async-start | bytes 6291456 | tf_op jit(solution)/shard_map/all_to_all | solution.py:188
  538.4 9.2 %copy-start.2 = (bf16[256,2048]{1,0:T(8,128)(2,1)S(1)}, bf16[256,2048]{1,0:T(8,128)(2,1)}, u32[]{:S(2)}) copy-start(bf16[256,2048]{1,0:T(8,128)(2,1)} %copy-done.1) | copy-start | bytes 3145732
  538.4 9.2 %copy-start.8 = (f32[2048]{0:T(1024)S(1)}, f32[2048]{0:T(1024)}, u32[]{:S(2)}) copy-start(f32[2048]{0:T(1024)} %param.45) | copy-start | bytes 24580
Sparse Core Ops, SparseCore 0:
  9.5 53.9 all-gather.9
  65.6 48.3 all-gather.7
  115.5 104.5 all-gather.5
